TPU v7x, 32 devices: a whole 2x2x4 slice. The times are simulated.
32 devices in a mesh: sp: 4 (over z), tp: 4 (over y, x), dp: 2 (over core).
Axes of the slice: x: 2, y: 2, z: 4, core: 2. Of those that a mesh axis runs over, the one named last changes fastest.
Arguments:
- latent: bfloat16 [2, 768, 2048], P('dp', 'sp'), may hold values from -6 to 6
- cond: bfloat16 [2, 2048], P('dp', 'sp'), may hold values from -6 to 6
- context: bfloat16 [2, 32, 2048], P('dp', 'sp'), may hold values from -6 to 6
- ctx_cond: bfloat16 [2048], P('sp'), may hold values from -6 to 6
- w_mod: bfloat16 [2048, 6144], P('sp', 'tp'), may hold values from -0.125 to 0.125
- norm_gain: bfloat16 [2048], replicated, may hold values from 0.099609375 to 1.8984375
- w_query: bfloat16 [2048, 1024], P(None, 'tp'), may hold values from -0.125 to 0.125
- w_key: bfloat16 [2048, 1024], P(None, 'tp'), may hold values from -0.125 to 0.125
- w_value: bfloat16 [2048, 1024], P(None, 'tp'), may hold values from -0.125 to 0.125
- w_outgate: bfloat16 [2048, 1024], P(None, 'tp'), may hold values from -0.125 to 0.125
- w_decay: bfloat16 [2048, 2, 8], P(None, None, 'tp'), may hold values from -0.125 to 0.125
- w_beta: bfloat16 [2048, 2, 8], P(None, None, 'tp'), may hold values from -0.125 to 0.125
- decay_rate: float32 [2, 8], P(None, 'tp'), may hold values from 6.510417e-05 to 0.0333333333
- decay_bias: float32 [2, 8], P(None, 'tp'), may hold values from -3 to 3
- extra_decay: float32 [2, 2, 8, 768], P('dp', None, 'tp', 'sp'), may hold values from -0.7007812 to -0.000130208333
- out_gain: bfloat16 [128], replicated, may hold values from 0.099609375 to 1.8984375
- w_out: bfloat16 [1024, 2048], replicated, may hold values from -0.1875 to 0.1875
Outputs:
- mixed_out: bfloat16 [2, 768, 2048], P('dp', ('sp', 'tp'))
All inputs are finite; a program needn't handle non-finite values.
Results may differ from a plain program's by a relative error of at most 0.0067.
Values may be sent and summed in bfloat16 or wider, within the bound.
A program may use at most 128 MiB of HBM per device.

v0:
```python
import jax
import jax.numpy as jnp
from jax import lax
from jax.sharding import PartitionSpec as P

D = 2048
HEAD = 128
BLOCK = 64


norm_eps = 1e-06
beta_scale = 30.0


def prefix_2(array, axis, combine, identity, reverse):
    devices, mine = (lax.axis_size(axis), lax.axis_index(axis))
    everything = jax.tree.map(lambda part: lax.all_gather(part, axis), array)
    start = jax.tree.map(
        lambda part, zero: jnp.broadcast_to(jnp.asarray(zero, part.dtype), part.shape),
        array,
        identity,
    )

    def turn(k, before):
        at = devices - 1 - k if reverse else k
        reached = at > mine if reverse else at < mine
        new = combine(before, jax.tree.map(lambda part: part[at], everything))
        return jax.tree.map(lambda a, b: jnp.where(reached, a, b), new, before)

    return lax.fori_loop(0, devices, turn, start)


def contract_product(einsum_form, left_op, right_op):
    return jnp.einsum(einsum_form, left_op, right_op, precision=lax.Precision.HIGHEST)


def less_product(base_value, einsum_form, left_op, right_op):
    product_value = lax.optimization_barrier(contract_product(einsum_form, left_op, right_op))
    return base_value - product_value


def modulate(rows_in, gain_vec, scale_row, shift_row):
    values = rows_in.astype(jnp.float32)
    normed = values * lax.rsqrt(jnp.mean(values * values, axis=-1, keepdims=True) + norm_eps)
    return (normed * gain_vec.astype(jnp.float32) * (1.0 + scale_row) + shift_row).astype(
        jnp.bfloat16
    )


def unit_normal(values):
    return values * lax.rsqrt(jnp.sum(values * values, axis=-1, keepdims=True) + norm_eps)


def head_view(raw_proj, head_count):
    return raw_proj.astype(jnp.float32).reshape(raw_proj.shape[0], head_count, -1)


def split_inputs(raw_proj, head_count, inner_width):
    row_count = raw_proj.shape[0]
    key_rows = unit_normal(jax.nn.silu(head_view(raw_proj[:, :inner_width], head_count)))
    value_rows = jax.nn.silu(head_view(raw_proj[:, inner_width : 2 * inner_width], head_count))
    decay_raw = raw_proj[:, 2 * inner_width : 2 * inner_width + 2 * head_count].astype(jnp.float32)
    beta_raw = raw_proj[:, 2 * inner_width + 2 * head_count :].astype(jnp.float32)
    return (
        key_rows,
        value_rows,
        decay_raw.reshape(row_count, 2, head_count),
        beta_raw.reshape(row_count, 2, head_count),
    )


def orient(values, direction):
    if direction:
        return values[::-1]
    return values


def to_blocks(values, block_width):
    block_count = values.shape[0] // block_width
    shaped = values.reshape((block_count, block_width) + values.shape[1:])
    return jnp.moveaxis(shaped, 2, 1)


def unit_inverse(lowpart, block_width):
    positions = jnp.arange(block_width)
    result = jnp.broadcast_to(jnp.eye(block_width, dtype=jnp.float32), lowpart.shape)
    for level_index in range((block_width - 1).bit_length()):
        half_width = 1 << level_index
        same_pair = positions[:, None] // (2 * half_width) == positions[None, :] // (2 * half_width)
        lower_half = positions[:, None] // half_width % 2 == 1
        upper_half = positions[None, :] // half_width % 2 == 0
        coupling = jnp.where(same_pair & lower_half & upper_half, lowpart, 0.0)
        inner_term = lax.optimization_barrier(contract_product("nhij,nhjk->nhik", coupling, result))
        result = less_product(result, "nhij,nhjk->nhik", result, inner_term)
    return result


def block_terms(key_rows, value_rows, log_decay, beta_rows, block_width):
    key_blocks = to_blocks(key_rows, block_width)
    value_blocks = to_blocks(value_rows, block_width)
    cumulative = jnp.cumsum(to_blocks(log_decay, block_width), axis=-1)
    beta_blocks = to_blocks(beta_rows, block_width)
    positions = jnp.arange(block_width)
    lower_mask = positions[:, None] >= positions[None, :]
    strict = positions[:, None] > positions[None, :]
    spread = cumulative[..., :, None] - cumulative[..., None, :]
    weights = jnp.where(lower_mask, jnp.exp(jnp.where(lower_mask, spread, 0.0)), 0.0)
    scaled = key_blocks * beta_blocks[..., None]
    lowpart = jnp.where(
        strict, contract_product("nhid,nhjd->nhij", scaled, key_blocks) * weights, 0.0
    )
    inverse = unit_inverse(lowpart, block_width)
    state_update = contract_product(
        "nhij,nhjd->nhid", inverse, value_blocks * beta_blocks[..., None]
    )
    erased_state = contract_product(
        "nhij,nhjd->nhid", inverse, scaled * jnp.exp(cumulative)[..., None]
    )
    final_log_decay = cumulative[..., -1]
    decayed_keys = key_blocks * jnp.exp(final_log_decay[..., None] - cumulative)[..., None]
    return (
        (state_update, erased_state, decayed_keys, final_log_decay),
        (key_blocks, cumulative, weights),
    )


def query_terms(queries, extras):
    key_blocks, cumulative, weights = extras
    query_blocks = to_blocks(queries, key_blocks.shape[2])
    query_decayed = query_blocks * jnp.exp(cumulative)[..., None]
    query_keys = contract_product("nhid,nhjd->nhij", query_blocks, key_blocks) * weights
    return (query_decayed, query_keys)


def direction_terms(
    key_rows, value_rows, decay_raw, beta_raw, decay_rate, decay_bias, direction, added, block_width
):
    log_decay = (
        -decay_rate[direction] * jax.nn.softplus(decay_raw[:, direction] + decay_bias[direction])
        + added
    )
    beta_rows = jax.nn.sigmoid(beta_raw[:, direction]) * (beta_scale * decay_rate[direction])
    return block_terms(
        orient(key_rows, direction),
        orient(value_rows, direction),
        orient(log_decay, direction),
        orient(beta_rows, direction),
        block_width,
    )


def carry_state(state_now, parts):

    def carry_advance(carried_state, inputs):
        state_update, erased_state, decayed_keys, final_log_decay = inputs
        new_value_rows = less_product(state_update, "tze,tem->tzm", erased_state, carried_state)
        carried_state = carried_state * jnp.exp(final_log_decay)[:, None, None] + contract_product(
            "rbz,rbi->rzi", decayed_keys, new_value_rows
        )
        return (carried_state, None)

    return lax.scan(carry_advance, state_now, parts)[0]


def span_map(parts, identity, zero_state):

    def span_advance(carried_state, inputs):
        state_update, erased_state, decayed_keys, final_log_decay = inputs
        step_matrix = less_product(
            jnp.exp(final_log_decay)[:, None, None] * identity,
            "hck,hcj->hkj",
            decayed_keys,
            erased_state,
        )
        span_matrix = contract_product("hij,hjk->hik", step_matrix, carried_state[0])
        span_offset = contract_product(
            "bgd,bdc->bgc", step_matrix, carried_state[1]
        ) + contract_product("rbz,rbi->rzi", decayed_keys, state_update)
        return ((span_matrix, span_offset), None)

    return lax.scan(span_advance, (identity, zero_state), parts)[0]


def compose(earlier, later):
    return (
        contract_product("hij,hjk->hik", later[0], earlier[0]),
        contract_product("bgd,bdc->bgc", later[0], earlier[1]) + later[1],
    )


def read_out(state_now, parts, query_decayed, query_keys):

    def read_advance(carried_state, inputs):
        state_update, erased_state, decayed_keys, final_log_decay, query_tile, query_matrix = inputs
        new_value_rows = less_product(state_update, "tze,tem->tzm", erased_state, carried_state)
        state_readout = contract_product(
            "tze,tem->tzm", query_tile, carried_state
        ) + contract_product("bgd,bdc->bgc", query_matrix, new_value_rows)
        carried_state = carried_state * jnp.exp(final_log_decay)[:, None, None] + contract_product(
            "rbz,rbi->rzi", decayed_keys, new_value_rows
        )
        return (carried_state, state_readout)

    readouts = lax.scan(read_advance, state_now, parts + (query_decayed, query_keys))[1]
    block_count, head_count, block_width, value_width = readouts.shape
    return jnp.moveaxis(readouts, 1, 2).reshape(block_count * block_width, head_count, value_width)


def on_device(
    latent,
    cond,
    context,
    ctx_cond,
    w_mod,
    norm_gain,
    w_query,
    w_key,
    w_value,
    w_outgate,
    w_decay,
    w_beta,
    decay_rate,
    decay_bias,
    extra_decay,
    out_gain,
    w_out,
):
    head_count = w_decay.shape[2]
    inner_width = head_count * HEAD
    span_len = latent.shape[1]
    tp_count = lax.axis_size("tp")
    rows_out = span_len // tp_count
    cond_all = jnp.concatenate([cond, ctx_cond[None, :]], axis=0)
    cond_rows = jax.nn.silu(cond_all.astype(jnp.float32)).astype(jnp.bfloat16)
    partial_mod = jnp.dot(cond_rows, w_mod, preferred_element_type=jnp.float32)
    summed = lax.psum(partial_mod, "sp")
    modulation = lax.all_gather(summed, "tp", axis=1, tiled=True)
    shift_rows = modulation[:, :D]
    scale_rows = modulation[:, D : 2 * D]
    gate_rows = modulation[:, 2 * D :]
    ctx_joined = jnp.concatenate(
        [w_key, w_value, w_decay.reshape(D, 2 * head_count), w_beta.reshape(D, 2 * head_count)],
        axis=1,
    )
    lat_joined = jnp.concatenate([w_query, w_outgate, ctx_joined], axis=1)
    identity = jnp.broadcast_to(jnp.eye(HEAD, dtype=jnp.float32), (head_count, HEAD, HEAD))
    zero_state = jnp.zeros((head_count, HEAD, HEAD), jnp.float32)
    ctx_in = modulate(context[0], norm_gain, scale_rows[1], shift_rows[1])
    ctx_proj = jnp.dot(
        lax.all_gather(ctx_in, "sp", axis=0, tiled=True),
        ctx_joined,
        preferred_element_type=jnp.float32,
    ).astype(jnp.bfloat16)
    ctx_block = min(BLOCK, ctx_proj.shape[0])
    lat_in = modulate(latent[0], norm_gain, scale_rows[0], shift_rows[0])
    lat_proj = jnp.dot(lat_in, lat_joined, preferred_element_type=jnp.float32).astype(jnp.bfloat16)
    queries = unit_normal(jax.nn.silu(head_view(lat_proj[:, :inner_width], head_count))) * HEAD ** (
        -0.5
    )
    outgate = lat_proj[:, inner_width : 2 * inner_width]
    ctx_inputs = split_inputs(ctx_proj, head_count, inner_width)
    lat_inputs = split_inputs(lat_proj[:, 2 * inner_width :], head_count, inner_width)
    summed_out = jnp.zeros((span_len, head_count, HEAD), jnp.float32)
    for direction in range(2):
        ctx_parts = direction_terms(*ctx_inputs, decay_rate, decay_bias, direction, 0.0, ctx_block)[
            0
        ]
        ctx_state = carry_state(zero_state, ctx_parts)
        lat_parts, extras = direction_terms(
            *lat_inputs, decay_rate, decay_bias, direction, extra_decay[0, direction].T, BLOCK
        )
        span_pair = span_map(lat_parts, identity, zero_state)
        if direction == 0:
            prefix = prefix_2(span_pair, "sp", compose, (identity, zero_state), False)
        else:
            prefix = prefix_2(span_pair, "sp", compose, (identity, zero_state), True)
        state_now = contract_product("bgd,bdc->bgc", prefix[0], ctx_state) + prefix[1]
        query_decayed, query_keys = query_terms(orient(queries, direction), extras)
        summed_out = summed_out + orient(
            read_out(state_now, lat_parts, query_decayed, query_keys), direction
        )
    normed = summed_out * lax.rsqrt(
        jnp.mean(summed_out * summed_out, axis=-1, keepdims=True) + norm_eps
    )
    normed = normed * out_gain.astype(jnp.float32)
    gated = (
        (normed * jax.nn.silu(head_view(outgate, head_count)))
        .reshape(span_len, inner_width)
        .astype(jnp.bfloat16)
    )
    by_rows = lax.all_to_all(gated, "tp", split_axis=0, concat_axis=1, tiled=True)
    mixed_rows = jnp.dot(by_rows, w_out, preferred_element_type=jnp.float32)
    own_rows = lax.dynamic_slice_in_dim(latent[0], lax.axis_index("tp") * rows_out, rows_out, 0)
    return (own_rows.astype(jnp.float32) + gate_rows[0] * mixed_rows).astype(jnp.bfloat16)[None]


def solution(mesh):
    placed = (
        P("dp", "sp", None),
        P("dp", "sp"),
        P("dp", "sp", None),
        P("sp"),
        P("sp", "tp"),
        P(),
        P(None, "tp"),
        P(None, "tp"),
        P(None, "tp"),
        P(None, "tp"),
        P(None, None, "tp"),
        P(None, None, "tp"),
        P(None, "tp"),
        P(None, "tp"),
        P("dp", None, "tp", "sp"),
        P(),
        P(),
    )
    return jax.shard_map(
        on_device,
        mesh=mesh,
        in_specs=placed,
        out_specs=P("dp", ("sp", "tp"), None),
        check_vma=False,
    )
```

profile of v0, /device:TPU:0, one launch (start us, length us, event | category | flops | bytes accessed | tf_op | source)
XLA Modules:
  0.0 255.0 jit_solution(1076202069718715104)
XLA Ops:
  2.4 20.4 %psum.7 = f32[2,1536]{1,0:T(2,128)S(1)} all-reduce(f32[2,1536]{1,0:T(2,128)S(1)} %fusion.343), channel_id=1, replica_groups=mesh['sp'=4,'tp'=4,'dp'=2] {'sp'}, use_global_device_ids=true, to_apply=%region_0.1 | all-reduce | flops 3072 | bytes 24576 | tf_op jit(solution)/shard_map/psum | solution.py:236
  22.9 8.2 %all_gather.30 = f32[2,6144]{1,0:T(2,128)S(1)} all-gather(f32[2,1536]{1,0:T(2,128)S(1)} %psum.7), channel_id=1, replica_groups=mesh['sp'=4,'tp'=4,'dp'=2] {'tp'}, dimensions={1}, use_global_device_ids=true | all-gather | bytes 61440 | tf_op jit(solution)/shard_map/all_gather | solution.py:237
  34.1 14.1 %all_gather.35 = bf16[32,2048]{1,0:T(8,128)(2,1)} all-gather(bf16[8,2048]{1,0:T(8,128)(2,1)S(1)} %fusion.222), channel_id=1, replica_groups=mesh['sp'=4,'tp'=4,'dp'=2] {'sp'}, dimensions={0}, use_global_device_ids=true | all-gather | bytes 163840 | tf_op jit(solution)/shard_map/all_gather | solution.py:250
  49.7 3.0 %fusion.121 = bf16[32,520]{0,1:T(8,128)(2,1)S(1)} fusion(bf16[32,2048]{1,0:T(8,128)(2,1)} %all_gather.35, bf16[2048,4]{1,0:T(8,128)(2,1)S(1)} %copy.281, bf16[2048,4]{1,0:T(8,128)(2,1)S(1)} %copy.280, bf16[2048,256]{1,0:T(8,128)(2,1)} %param.37, bf16[2048,256]{1,0:T(8,128)(2,1)} %param.36), kind=kOutput, calls=%fused_computation.143 | convolution fusion | flops 76693760 | bytes 2294272 | tf_op jit(solution)/shard_map/dot_general | solution.py:249
  60.6 8.0 %concatenate.11 = bf16[2048,1032]{1,0:T(8,128)(2,1)} concatenate(bf16[2048,256]{1,0:T(8,128)(2,1)} %param.35, bf16[2048,256]{1,0:T(8,128)(2,1)} %param.38, bf16[2048,256]{1,0:T(8,128)(2,1)} %param.36, bf16[2048,256]{1,0:T(8,128)(2,1)} %param.37, bf16[2048,4]{1,0:T(8,128)(2,1)S(1)} %copy.280, bf16[2048,4]{1,0:T(8,128)(2,1)S(1)} %copy.281), dimensions={1} | concatenate | bytes 8454144 | tf_op jit(solution)/shard_map/concatenate | solution.py:245
  68.5 4.3 %convolution_convert_fusion = bf16[192,1032]{0,1:T(8,128)(2,1)S(1)} fusion(bf16[2048,1032]{1,0:T(8,128)(2,1)} %concatenate.11, bf16[1,192,2048]{2,1,0:T(8,128)(2,1)S(1)} %copy-done.5, f32[2048]{0:T(1024)S(1)} %bitcast.615, f32[2048]{0:T(1024)S(1)} %bitcast.616, f32[2048]{0:T(1024)S(1)} %convert_element_type.121, f32[192]{0:T(256)S(1)} %add_rsqrt_fusion.4), kind=kOutput, calls=%fused_computation.131 | convolution fusion | flops 814155264 | bytes 5435136 | tf_op jit(solution)/shard_map/dot_general | solution.py:256
  100.8 1.8 reverse.3
  104.4 1.8 rev.33
  114.3 1.7 reshape.1942
  116.8 3.2 %broadcast_multiply_fusion.8 = (f32[3,2,64,128]{3,1,2,0:T(2,128)}, f32[3,2,64,128]{3,1,2,0:T(2,128)}, f32[3,2,64,128]{3,1,2,0:T(2,128)S(1)}, f32[3,2,64,128]{3,1...) fusion(f32[3,2,64]{1,2,0:T(8,128)} %copy.294, f32[3,64,2]{2,1,0:T(8,128)} %bitcast.603, ...), kind=kLoop, calls=%fused_computation.260 | loop fusion | flops 933888 | bytes 1775616 | tf_op jit(solution)/shard_map/mul | solution.py:130
  127.7 6.5 %while.94 = (s32[]{:T(128)}, f32[2,128,128]{2,1,0:T(8,128)S(1)}, f32[2,128,128]{2,1,0:T(8,128)S(1)}, f32[3,2]{1,0:T(4,128)}, f32[3,2,64,128]{3,2,1,0:T(8,128)S(1...) while((s32[]{:T(128)}, f32[2,128,128]{2,1,0:T(8,128)S(1)}, ...), condition=%wide.region_5.6_spmd.clone, body=%wide.region_4.5_spmd.clone.sunk | while | flops 151191552 | bytes 1837203 | solution.py:181
  134.9 15.0 %all-gather = f32[8,128,128]{2,1,0:T(8,128)S(1)} all-gather(f32[2,128,128]{2,1,0:T(8,128)S(1)} %get-tuple-element.486), channel_id=2, replica_groups=mesh['sp'=4,'tp'=4,'dp'=2] {'sp'}, dimensions={0}, use_global_device_ids=true | all-gather | bytes 655360 | tf_op jit(solution)/shard_map/all_gather | solution.py:17
  149.9 15.4 %all-gather.1 = f32[8,128,128]{2,1,0:T(8,128)} all-gather(f32[2,128,128]{2,1,0:T(8,128)S(1)} %get-tuple-element.487), channel_id=3, replica_groups=mesh['sp'=4,'tp'=4,'dp'=2] {'sp'}, dimensions={0}, use_global_device_ids=true | all-gather | bytes 655360 | tf_op jit(solution)/shard_map/all_gather | solution.py:17
  165.3 6.1 %while.95 = (s32[]{:T(128)}, f32[2,128,128]{2,1,0:T(8,128)S(1)}, f32[2,128,128]{2,1,0:T(8,128)S(1)}, s32[]{:T(128)}, f32[4,2,128,128]{3,2,1,0:T(8,128)S(1)}, /*i...) while((s32[]{:T(128)}, f32[2,128,128]{2,1,0:T(8,128)S(1)}, f32[2,128,128]{2,1,0:T(8,128)S(1)}, ...), condition=%wide.region_7.8_spmd.clone, body=%wide.region_6.7_spmd.clone.sunk | while | flops 100827136 | bytes 1706604 | solution.py:30
  171.5 1.4 convolution_multiply_fusion.3
  175.5 10.6 %while.92 = (s32[]{:T(128)}, f32[2,128,128]{2,1,0:T(8,128)S(1)}, f32[3,2,64,128]{3,2,0,1:T(8,128)S(1)}, f32[3,2]{1,0:T(4,128)}, f32[3,2,64,128]{3,2,1,0:T(8,128)...) while((s32[]{:T(128)}, f32[2,128,128]{2,1,0:T(8,128)S(1)}, ...), condition=%wide.region_13.14_spmd, body=%wide.region_12.13_spmd.sunk | while | flops 88195072 | bytes 1445501 | solution.py:204
  192.6 4.5 %while.96 = (s32[]{:T(128)}, f32[2,128,128]{2,1,0:T(8,128)S(1)}, f32[2,128,128]{2,1,0:T(8,128)S(1)}, f32[3,2]{1,0:T(4,128)S(1)}, f32[3,2,64,128]{3,2,1,0:T(8,128...) while((s32[]{:T(128)}, f32[2,128,128]{2,1,0:T(8,128)S(1)}, ...), condition=%wide.region_16.17_spmd.clone, body=%wide.region_15.16_spmd.clone.sunk | while | flops 151191552 | bytes 1837203 | solution.py:181
  197.1 15.9 %all-gather.2 = f32[8,128,128]{2,1,0:T(8,128)S(1)} all-gather(f32[2,128,128]{2,1,0:T(8,128)S(1)} %get-tuple-element.491), channel_id=4, replica_groups=mesh['sp'=4,'tp'=4,'dp'=2] {'sp'}, dimensions={0}, use_global_device_ids=true | all-gather | bytes 655360 | tf_op jit(solution)/shard_map/all_gather | solution.py:17
  213.0 14.7 %all-gather.3 = f32[8,128,128]{2,1,0:T(8,128)S(1)} all-gather(f32[2,128,128]{2,1,0:T(8,128)S(1)} %get-tuple-element.492), channel_id=5, replica_groups=mesh['sp'=4,'tp'=4,'dp'=2] {'sp'}, dimensions={0}, use_global_device_ids=true | all-gather | bytes 655360 | tf_op jit(solution)/shard_map/all_gather | solution.py:17
  227.8 2.5 while.97
  232.9 8.5 %while.93 = (s32[]{:T(128)}, f32[2,128,128]{2,1,0:T(8,128)S(1)}, f32[3,2,64,128]{3,2,0,1:T(8,128)S(1)}, f32[3,2]{1,0:T(4,128)S(1)}, f32[3,2,64,128]{3,2,1,0:T(8,...) while((s32[]{:T(128)}, f32[2,128,128]{2,1,0:T(8,128)S(1)}, ...), condition=%wide.region_21.22_spmd, body=%wide.region_20.21_spmd.sunk | while | flops 88195072 | bytes 1314429 | solution.py:204
  243.1 3.3 %all-to-all-start = ((bf16[4,48,256]{2,1,0:T(8,128)(2,1)}), bf16[4,48,256]{2,1,0:T(8,128)(2,1)S(1)}, u32[]{:S(2)}, u32[]{:S(2)}) async-start(bf16[4,48,256]{2,1,0:T(8,128)(2,1)} %convert_element_type.137), calls=%async_computation | async-start | bytes 196608 | tf_op jit(solution)/shard_map/all_to_all | solution.py:291
  246.4 4.9 %all-to-all-done = bf16[4,48,256]{2,1,0:T(8,128)(2,1)S(1)} async-done(((bf16[4,48,256]{2,1,0:T(8,128)(2,1)}), bf16[4,48,256]{2,1,0:T(8,128)(2,1)S(1)}, u32[]{:S(2)}, u32[]{:S(2)}) %all-to-all-start) | async-done | bytes 98336 | tf_op jit(solution)/shard_map/all_to_all | solution.py:291
  251.3 3.7 %fusion.115 = bf16[1,48,2048]{2,1,0:T(8,128)(2,1)} fusion(bf16[48,1024]{1,0:T(8,128)(2,1)S(1)} %bitcast.605, bf16[1024,2048]{1,0:T(8,128)(2,1)} %param.45, f32[2048]{0:T(1024)S(1)} %bitcast.606, bf16[1,192,2048]{2,1,0:T(8,128)(2,1)} %param.29, s32[]{:T(128)S(6)} %select_n.815), kind=kOutput, calls=%fused_computation.135 | convolution fusion | flops 201719808 | bytes 4694020 | tf_op jit(solution)/shard_map/dot_general | solution.py:292
  (497 shorter events, 111.2 us)
Async XLA Ops:
  0.0 49.3 %copy-start.38 = (bf16[2048,2,2]{0,2,1:T(2,128)(2,1)S(1)}, bf16[2048,2,2]{0,2,1:T(2,128)(2,1)}, u32[]{:S(2)}) copy-start(bf16[2048,2,2]{0,2,1:T(2,128)(2,1)} %param.40) | copy-start | bytes 49156
  58.6 25.8 %copy-start.50 = (f32[2]{0:T(128)}, f32[2]{0:T(128)S(1)}, u32[]{:S(2)}) copy-start(f32[2]{0:T(128)S(1)} %get-tuple-element.936) | copy-start | bytes 28
  58.6 25.8 %copy-start.52 = (f32[2]{0:T(128)}, f32[2]{0:T(128)S(1)}, u32[]{:S(2)}) copy-start(f32[2]{0:T(128)S(1)} %get-tuple-element.937) | copy-start | bytes 28
  58.6 30.5 %copy-start.46 = (f32[2]{0:T(128)}, f32[2]{0:T(128)S(1)}, u32[]{:S(2)}) copy-start(f32[2]{0:T(128)S(1)} %get-tuple-element.935) | copy-start | bytes 28
  58.6 25.7 %copy-start.54 = (f32[2]{0:T(128)}, f32[2]{0:T(128)S(1)}, u32[]{:S(2)}) copy-start(f32[2]{0:T(128)S(1)} %get-tuple-element.940) | copy-start | bytes 28
  72.8 13.5 %copy-start.8 = (f32[32,256]{0,1:T(8,128)S(1)}, f32[32,256]{0,1:T(8,128)}, u32[]{:S(2)}) copy-start(f32[32,256]{0,1:T(8,128)} %get-tuple-element.909) | copy-start | bytes 98308
  74.2 45.9 %copy-start.30 = (pred[64,64]{1,0:T(8,128)(4,1)}, pred[64,64]{1,0:T(8,128)(4,1)S(1)}, u32[]{:S(2)}) copy-start(pred[64,64]{1,0:T(8,128)(4,1)S(1)} %get-tuple-element.946) | copy-start | bytes 12292
  77.0 19.6 %copy-start.6 = (f32[32,256]{0,1:T(8,128)S(1)}, f32[32,256]{0,1:T(8,128)}, u32[]{:S(2)}) copy-start(f32[32,256]{0,1:T(8,128)} %get-tuple-element.908) | copy-start | bytes 98308
  84.4 12.9 %copy-start.51 = (f32[2]{0:T(128)S(1)}, f32[2]{0:T(128)}, u32[]{:S(2)}) copy-start(f32[2]{0:T(128)} %copy-done.50) | copy-start | bytes 28
  84.4 12.9 %copy-start.53 = (f32[2]{0:T(128)S(1)}, f32[2]{0:T(128)}, u32[]{:S(2)}) copy-start(f32[2]{0:T(128)} %copy-done.52) | copy-start | bytes 28
  84.5 12.9 %copy-start.55 = (f32[2]{0:T(128)S(1)}, f32[2]{0:T(128)}, u32[]{:S(2)}) copy-start(f32[2]{0:T(128)} %copy-done.54) | copy-start | bytes 28
  86.5 13.9 %copy-start.58 = (f32[32,2]{0,1:T(2,128)}, f32[32,2]{0,1:T(2,128)S(1)}, u32[]{:S(2)}) copy-start(f32[32,2]{0,1:T(2,128)S(1)} %add_rsqrt_fusion.3) | copy-start | bytes 772
  89.1 11.2 %copy-start.68 = (f32[2,32]{1,0:T(2,128)}, f32[2,32]{1,0:T(2,128)S(1)}, u32[]{:S(2)}) copy-start(f32[2,32]{1,0:T(2,128)S(1)} %fusion.377) | copy-start | bytes 772
  93.4 15.1 %copy-start.31 = (pred[32,32]{1,0:T(8,128)(4,1)}, pred[32,32]{1,0:T(8,128)(4,1)S(1)}, u32[]{:S(2)}) copy-start(pred[32,32]{1,0:T(8,128)(4,1)S(1)} %and_and_fusion.7) | copy-start | bytes 3076
  93.8 14.7 %copy-start.18 = (f32[1,2,32,32]{3,2,1,0:T(8,128)}, f32[1,2,32,32]{3,2,1,0:T(8,128)S(1)}, u32[]{:S(2)}) copy-start(f32[1,2,32,32]{3,2,1,0:T(8,128)S(1)} %sub.500) | copy-start | bytes 24580
  94.6 13.9 %copy-start.33 = (pred[32,32]{1,0:T(8,128)(4,1)}, pred[32,32]{1,0:T(8,128)(4,1)S(1)}, u32[]{:S(2)}) copy-start(pred[32,32]{1,0:T(8,128)(4,1)S(1)} %and_and_fusion.6) | copy-start | bytes 3076
  97.3 11.2 %copy-start.42 = (pred[64,64]{1,0:T(8,128)(4,1)S(1)}, pred[64,64]{1,0:T(8,128)(4,1)}, u32[]{:S(2)}) copy-start(pred[64,64]{1,0:T(8,128)(4,1)} %get-tuple-element.947) | copy-start | bytes 12292
  175.4 11.4 %copy-start.34 = (pred[32,32]{1,0:T(8,128)(4,1)S(1)}, pred[32,32]{1,0:T(8,128)(4,1)}, u32[]{:S(2)}) copy-start(pred[32,32]{1,0:T(8,128)(4,1)} %copy-done.33) | copy-start | bytes 3076
  175.4 11.7 %copy-start.23 = (f32[32,2,128]{2,0,1:T(8,128)S(1)}, f32[32,2,128]{2,0,1:T(8,128)}, u32[]{:S(2)}) copy-start(f32[32,2,128]{2,0,1:T(8,128)} %copy-done.22) | copy-start | bytes 98308
  175.5 11.7 %copy-start.40 = (f32[32,2]{0,1:T(2,128)S(1)}, f32[32,2]{0,1:T(2,128)}, u32[]{:S(2)}) copy-start(f32[32,2]{0,1:T(2,128)} %copy-done.39) | copy-start | bytes 772
  175.5 11.7 %copy-start.57 = (f32[2,32]{1,0:T(2,128)S(1)}, f32[2,32]{1,0:T(2,128)}, u32[]{:S(2)}) copy-start(f32[2,32]{1,0:T(2,128)} %get-tuple-element.942) | copy-start | bytes 772
  175.5 12.8 %copy-start.7 = (f32[32,256]{0,1:T(8,128)S(1)}, f32[32,256]{0,1:T(8,128)}, u32[]{:S(2)}) copy-start(f32[32,256]{0,1:T(8,128)} %get-tuple-element.908) | copy-start | bytes 98308
  175.5 13.5 %copy-start.2 = (f32[3,2,64,64]{3,2,1,0:T(8,128)S(1)}, f32[3,2,64,64]{3,2,1,0:T(8,128)}, u32[]{:S(2)}) copy-start(f32[3,2,64,64]{3,2,1,0:T(8,128)} %get-tuple-element.922) | copy-start | bytes 294916
  243.1 8.2 %all-to-all-start = ((bf16[4,48,256]{2,1,0:T(8,128)(2,1)}), bf16[4,48,256]{2,1,0:T(8,128)(2,1)S(1)}, u32[]{:S(2)}, u32[]{:S(2)}) async-start(bf16[4,48,256]{2,1,0:T(8,128)(2,1)} %convert_element_type.137), calls=%async_computation | async-start | bytes 196608 | tf_op jit(solution)/shard_map/all_to_all | solution.py:291
  (60 other events, 307.1 us)
where the time goes:
time: 258 us; the launch traced here: 255 us
  blocking collectives  104 us (40%)
  matrix products  68.8 us (27%)
  local copies, waits for them, and re-layouts  36.3 us (14%)
  other arithmetic  35 us (14%)
  waiting for transfers between devices  4.89 us (2%)
  starting transfers between devices  3.3 us (1%)
    all_gather x4, blocking collectives, prefix_2(): everything = jax.tree.map(lambda part: lax.all_gather(part, axis), array)  60.9 us
    dot_general x128, matrix products, contract_product(): jnp.einsum(einsum_form, left_op, right_op, precision=lax.Precision.HIGHEST)  56.8 us
    psum x1, blocking collectives, on_device(): summed = lax.psum(partial_mod, 'sp')  20.4 us
    all_gather x1, blocking collectives, on_device(): lax.all_gather(ctx_in, 'sp', axis=0, tiled=True)  14.1 us
    all_gather x1, blocking collectives, on_device(): modulation = lax.all_gather(summed, 'tp', axis=1, tiled=True)  8.23 us
    concatenate x1, local copies, waits for them, and re-layouts, on_device(): lat_joined = jnp.concatenate([w_query, w_outgate, ctx_joined], axis=1)  7.98 us
    eq x11, other arithmetic, unit_inverse(): upper_half = positions[None, :] // half_width % 2 == 0  5.74 us
    select_n x11, other arithmetic, unit_inverse(): positions[:, None] // (2 * half_width)  5.41 us
  transfers between devices with their start and end apart: 1, of which 1 were waited for; matrix products, arithmetic and copies ran while one was open for 0% of the time, Pallas kernels for 0%

commit v1 on v0

v1 whole, which is shorter than its diff:
```python
import functools

import jax
import jax.numpy as jnp
from jax import lax
from jax.experimental import pallas as pl
from jax.experimental.pallas import tpu as pltpu
from jax.sharding import PartitionSpec as P

HEAD = 128
norm_eps = 1e-06
beta_scale = 30.0
MESH = pl.DeviceIdType.MESH
F32 = jnp.float32
BF16 = jnp.bfloat16


def mm(a, b):
    return jnp.dot(a.astype(BF16), b.astype(BF16), preferred_element_type=F32)


def mm_nt(a, b):
    return lax.dot_general(
        a.astype(BF16), b.astype(BF16), (((1,), (1,)), ((), ())), preferred_element_type=F32
    )


def silu(v):
    return v / (1.0 + jnp.exp(-v))


def unit_normal(u):
    return u * lax.rsqrt(jnp.sum(u * u, axis=-1, keepdims=True) + norm_eps)


def softplus(v):
    return jnp.maximum(v, 0.0) + jnp.log1p(jnp.exp(-jnp.abs(v)))


def kernel(
    n,
    t,
    heads,
    rate_ref,
    bias_ref,
    cond_ref,
    ctx_cond_ref,
    context_ref,
    gain_ref,
    out_gain_ref,
    wdb_ref,
    extra_ref,
    latent_hbm,
    w_mod_hbm,
    w_query_hbm,
    w_outgate_hbm,
    w_key_hbm,
    w_value_hbm,
    w_out_hbm,
    out_ref,
    lat_v,
    wm_v,
    w_v,
    wout_v,
    ctx_all,
    mod_part,
    mod_full,
    xin,
    ext_v,
    own_a,
    own_b,
    pre_a,
    pre_b,
    send_map,
    recv_map,
    gated_v,
    gated_r,
    load_sem,
    ctx_send,
    ctx_recv,
    part_send,
    part_recv,
    full_send,
    full_recv,
    map_send,
    map_recv,
    gate_send,
    gate_recv,
):
    sp = lax.axis_index("sp")
    tp = lax.axis_index("tp")
    span = lat_v.shape[0]
    depth = lat_v.shape[1]
    rows = xin.shape[0]
    ctx_len = n * context_ref.shape[1]
    inner = heads * HEAD
    chains = 2 * heads
    rows_out = span // t

    def load(i, src, dst):
        copy = pltpu.make_async_copy(src, dst, load_sem.at[i])
        copy.start()
        return copy

    load_mod = load(0, w_mod_hbm, wm_v)
    load_lat = load(1, latent_hbm.at[0], lat_v)
    load_w = [
        load(2 + i, w, w_v.at[i])
        for i, w in enumerate((w_key_hbm, w_value_hbm, w_query_hbm, w_outgate_hbm))
    ]
    load_out = load(6, w_out_hbm, wout_v)

    barrier = pltpu.get_barrier_semaphore()
    for k in range(1, n):
        pl.semaphore_signal(
            barrier, inc=1, device_id={"sp": lax.rem(sp + k, n)}, device_id_type=MESH
        )
    for k in range(1, t):
        pl.semaphore_signal(
            barrier, inc=1, device_id={"tp": lax.rem(tp + k, t)}, device_id_type=MESH
        )
    pl.semaphore_wait(barrier, n + t - 2)

    def spread(axis, me, count, src, dst, send, recv):
        sent = []
        for k in range(1, count):
            copy = pltpu.make_async_remote_copy(
                src_ref=src,
                dst_ref=dst.at[me],
                send_sem=send.at[k],
                recv_sem=recv.at[k],
                device_id={axis: lax.rem(me + k, count)},
                device_id_type=MESH,
            )
            copy.start()
            sent.append(copy)
        return sent

    def collect(axis, me, count, dst, send, recv):
        for k in range(1, count):
            slot = dst.at[lax.rem(me + count - k, count)]
            pltpu.make_async_remote_copy(
                src_ref=slot,
                dst_ref=slot,
                send_sem=send.at[k],
                recv_sem=recv.at[k],
                device_id={axis: lax.rem(me + k, count)},
                device_id_type=MESH,
            ).wait_recv()

    ctx_sent = spread("sp", sp, n, context_ref.at[0], ctx_all, ctx_send, ctx_recv)
    ctx_all[sp] = context_ref[0]

    pick = lax.broadcasted_iota(jnp.int32, (8, 1), 0)
    cond_f = silu(cond_ref[...].astype(F32))
    ctx_cond_f = silu(ctx_cond_ref[...].astype(F32))
    cond_rows = jnp.where(pick == 0, cond_f, jnp.where(pick == 1, ctx_cond_f, 0.0)).astype(BF16)
    load_mod.wait()
    part = jnp.dot(cond_rows, wm_v[...], preferred_element_type=F32)
    mod_part[sp] = part[:2]
    part_sent = spread("sp", sp, n, mod_part.at[sp], mod_part, part_send, part_recv)

    load_lat.wait()
    lat = lat_v[...].astype(F32)
    lat_r = lax.rsqrt(jnp.mean(lat * lat, axis=-1, keepdims=True) + norm_eps)
    collect("sp", sp, n, ctx_all, ctx_send, ctx_recv)
    ctx = ctx_all[...].astype(F32).reshape(ctx_len, depth)
    ctx_r = lax.rsqrt(jnp.mean(ctx * ctx, axis=-1, keepdims=True) + norm_eps)
    gain = gain_ref[...].astype(F32)
    if rows > span + ctx_len:
        xin[span + ctx_len :, :] = jnp.zeros((rows - span - ctx_len, depth), BF16)
    ext_v[...] = jnp.zeros(ext_v.shape, F32)
    for d in range(2):
        ext_v[d * heads : (d + 1) * heads, :span] = extra_ref[0, d]

    collect("sp", sp, n, mod_part, part_send, part_recv)
    summed = mod_part[0]
    for j in range(1, n):
        summed = summed + mod_part[j]
    mod_full[tp] = summed
    full_sent = spread("tp", tp, t, mod_full.at[tp], mod_full, full_send, full_recv)

    at_row = lax.broadcasted_iota(jnp.int32, (rows, rows), 0)
    at_col = lax.broadcasted_iota(jnp.int32, (rows, rows), 1)
    same = (at_row < span) == (at_col < span)
    lane = lax.broadcasted_iota(jnp.int32, (1, rows), 1)
    is_lat = lane < span
    is_ctx = jnp.logical_and(lane >= span, lane < span + ctx_len)

    collect("tp", tp, t, mod_full, full_send, full_recv)
    modulation = jnp.concatenate([mod_full[j] for j in range(t)], axis=1)
    shift = modulation[:, :depth]
    scale = gain * (1.0 + modulation[:, depth : 2 * depth])
    gate = modulation[0:1, 2 * depth :]
    xin[:span, :] = (lat_v[...].astype(F32) * lat_r * scale[0:1] + shift[0:1]).astype(BF16)
    ctx = ctx_all[...].astype(F32).reshape(ctx_len, depth)
    xin[span : span + ctx_len, :] = (ctx * ctx_r * scale[1:2] + shift[1:2]).astype(BF16)

    raw_t = lax.dot_general(
        wdb_ref[...], xin[...], (((1,), (1,)), ((), ())), preferred_element_type=F32
    ).astype(BF16).astype(F32)

    def project(i):
        load_w[i].wait()
        return jnp.dot(xin[...], w_v[i], preferred_element_type=F32).astype(BF16).astype(F32)

    chain = lax.broadcasted_iota(jnp.int32, (chains, 1), 0)
    rate = jnp.zeros((chains, 1), F32)
    bias = jnp.zeros((chains, 1), F32)
    for c in range(chains):
        rate = jnp.where(chain == c, rate_ref[c // heads, c % heads], rate)
        bias = jnp.where(chain == c, bias_ref[c // heads, c % heads], bias)
    g = -rate * softplus(raw_t[:chains] + bias) + ext_v[:chains, :]
    g = jnp.where(jnp.logical_or(is_lat, is_ctx), g, 0.0)
    beta = beta_scale * rate / (1.0 + jnp.exp(-raw_t[chains : 2 * chains]))
    up_to = jnp.where(jnp.logical_and(same, at_row <= at_col), 1.0, 0.0)
    from_on = jnp.where(jnp.logical_and(same, at_row >= at_col), 1.0, 0.0)
    g_hi = g.astype(BF16).astype(F32)
    g_mid = (g - g_hi).astype(BF16).astype(F32)
    g_lo = g - g_hi - g_mid
    g_parts = jnp.concatenate([g_hi, g_mid, g_lo, jnp.zeros_like(g)], axis=0)
    sums_0 = mm(g_parts, up_to)
    sums_1 = mm(g_parts, from_on)

    def join(s):
        return s[:chains] + s[chains : 2 * chains] + s[2 * chains : 3 * chains]

    cum = jnp.where(chain < heads, join(sums_0), join(sums_1))
    tot_lat = jnp.sum(jnp.where(is_lat, g, 0.0), axis=-1, keepdims=True)
    tot_ctx = jnp.sum(jnp.where(is_ctx, g, 0.0), axis=-1, keepdims=True)
    to_end_lat = jnp.where(is_lat, jnp.exp(jnp.where(is_lat, tot_lat - cum, 0.0)), 0.0)
    to_end_ctx = jnp.where(is_ctx, jnp.exp(jnp.where(is_ctx, tot_ctx - cum, 0.0)), 0.0)
    through = jnp.exp(tot_lat)
    packed = jnp.concatenate(
        [cum, beta, jnp.zeros((HEAD - 2 * chains, rows), F32)], axis=0
    )
    cols = packed.T
    grow = jnp.exp(cols)

    key_raw, value_raw = project(0), project(1)
    keys, values, queries, keys_t = [], [], [], []
    for h in range(heads):
        part_h = slice(h * HEAD, (h + 1) * HEAD)
        k = unit_normal(silu(key_raw[:, part_h]))
        keys.append(k)
        keys_t.append(k.T)
        values.append(silu(value_raw[:, part_h]))
    kk = [mm_nt(k, k) for k in keys]

    tri = [at_row >= at_col, at_row <= at_col]
    weights, low, inv = [], [], []
    for c in range(chains):
        d, h = c // heads, c % heads
        mask = jnp.logical_and(same, tri[d])
        diff = cols[:, c : c + 1] - cum[c : c + 1, :]
        w = jnp.where(mask, jnp.exp(jnp.where(mask, diff, 0.0)), 0.0)
        weights.append(w)
        b = cols[:, chains + c : chains + c + 1]
        low.append(jnp.where(at_row != at_col, b * kk[h] * w, 0.0))
    half = 1
    while half < rows:
        pair = at_row // (2 * half) == at_col // (2 * half)
        cross = [
            jnp.logical_and(pair, jnp.logical_and(at_row // half % 2 == 1, at_col // half % 2 == 0)),
            jnp.logical_and(pair, jnp.logical_and(at_row // half % 2 == 0, at_col // half % 2 == 1)),
        ]
        coupling = [jnp.where(cross[c // heads], low[c], 0.0) for c in range(chains)]
        if half == 1:
            eye = jnp.where(at_row == at_col, 1.0, 0.0)
            inv = [eye - coupling[c] for c in range(chains)]
        else:
            inner_term = [mm(coupling[c], inv[c]) for c in range(chains)]
            inv = [inv[c] - mm(inv[c], inner_term[c]) for c in range(chains)]
        half *= 2

    eye_head = jnp.where(
        lax.broadcasted_iota(jnp.int32, (HEAD, HEAD), 0)
        == lax.broadcasted_iota(jnp.int32, (HEAD, HEAD), 1),
        1.0,
        0.0,
    )
    solved = []
    place = [sp, n - 1 - sp]
    for c in range(chains):
        d, h = c // heads, c % heads
        b = cols[:, chains + c : chains + c + 1]
        right = jnp.concatenate(
            [values[h] * b, keys[h] * (b * grow[:, c : c + 1])], axis=1
        )
        x = mm(inv[c], right)
        solved.append(x)
        ba = mm(keys_t[h] * to_end_lat[c : c + 1, :], x)
        ctx_state = mm(keys_t[h] * to_end_ctx[c : c + 1, :], x[:, :HEAD])
        a = eye_head * through[c : c + 1, :] - ba[:, HEAD:]
        b_map = ba[:, :HEAD]
        first = place[d] == 0
        own_a[c] = a
        own_b[c] = b_map
        pre_a[c] = jnp.where(first, 0.0, eye_head)
        pre_b[c] = jnp.where(first, ctx_state, 0.0)
        send_map[0, d, h] = jnp.where(first, 0.0, a).astype(BF16)
        send_map[0, d, heads + h] = (
            b_map + jnp.where(first, mm(a, ctx_state), 0.0)
        ).astype(BF16)

    def map_copy(level, d, k):
        wide = 1 << level
        low_at = heads if 2 * wide == n else 0
        part_of = pl.ds(low_at, 2 * heads - low_at)
        target = lax.rem(sp + k, n) if d == 0 else lax.rem(sp + n - k, n)
        return pltpu.make_async_remote_copy(
            src_ref=send_map.at[level, d, part_of],
            dst_ref=recv_map.at[level, d, part_of],
            send_sem=map_send.at[level, d, k],
            recv_sem=map_recv.at[level, d],
            device_id={"sp": target},
            device_id_type=MESH,
        )

    levels = (n - 1).bit_length()

    def send_level(level):
        wide = 1 << level
        for d in range(2):

            @pl.when(lax.rem(place[d], 2 * wide) == wide - 1)
            def _():
                if level:
                    for h in range(heads):
                        c = d * heads + h
                        a = own_a[c]
                        send_map[level, d, heads + h] = (
                            mm(a, pre_b[c]) + own_b[c]
                        ).astype(BF16)
                        if 2 * wide != n:
                            send_map[level, d, h] = mm(a, pre_a[c]).astype(BF16)
                for k in range(1, wide + 1):
                    map_copy(level, d, k).start()

    def recv_level(level):
        wide = 1 << level
        for d in range(2):

            @pl.when(lax.rem(place[d], 2 * wide) >= wide)
            def _():
                map_copy(level, d, 1).wait_recv()
                for h in range(heads):
                    c = d * heads + h
                    a = pre_a[c]
                    pre_b[c] = mm(a, recv_map[level, d, heads + h]) + pre_b[c]
                    if 2 * wide != n:
                        pre_a[c] = mm(a, recv_map[level, d, h])

    if levels:
        send_level(0)

    query_raw, outgate_raw = project(2), project(3)
    local, mixers = [], []
    for h in range(heads):
        part_h = slice(h * HEAD, (h + 1) * HEAD)
        q = unit_normal(silu(query_raw[:, part_h])) * HEAD ** (-0.5)
        qk = mm_nt(q, keys[h])
        read = [mm(qk * weights[d * heads + h], solved[d * heads + h]) for d in range(2)]
        local.append(read[0][:, :HEAD] + read[1][:, :HEAD])
        mixers.append(
            jnp.concatenate(
                [
                    q * grow[:, d * heads + h : d * heads + h + 1] - read[d][:, HEAD:]
                    for d in range(2)
                ],
                axis=1,
            )
        )

    out_gate = [silu(outgate_raw[:, h * HEAD : (h + 1) * HEAD]) for h in range(heads)]
    for level in range(levels):
        recv_level(level)
        if level + 1 < levels:
            send_level(level + 1)

    out_gain = out_gain_ref[...].astype(F32)
    for h in range(heads):
        state = jnp.concatenate([pre_b[h], pre_b[heads + h]], axis=0)
        o = local[h] + mm(mixers[h], state)
        normed = o * lax.rsqrt(jnp.mean(o * o, axis=-1, keepdims=True) + norm_eps)
        gated = (normed * out_gain * out_gate[h]).astype(BF16)
        for j in range(t):
            gated_v[j, :, h * HEAD : (h + 1) * HEAD] = gated[j * rows_out : (j + 1) * rows_out]

    gate_sent = []
    for k in range(1, t):
        target = lax.rem(tp + k, t)
        copy = pltpu.make_async_remote_copy(
            src_ref=gated_v.at[target],
            dst_ref=gated_r.at[tp],
            send_sem=gate_send.at[k],
            recv_sem=gate_recv.at[k],
            device_id={"tp": target},
            device_id_type=MESH,
        )
        copy.start()
        gate_sent.append(copy)
    gated_r[tp] = gated_v[tp]
    load_out.wait()
    collect("tp", tp, t, gated_r, gate_send, gate_recv)
    by_rows = jnp.concatenate([gated_r[j] for j in range(t)], axis=1)
    mixed = jnp.dot(by_rows, wout_v[...], preferred_element_type=F32)
    own_rows = lat_v[pl.ds(pl.multiple_of(tp * rows_out, rows_out), rows_out), :].astype(F32)
    out_ref[0] = (own_rows + gate * mixed).astype(out_ref.dtype)

    for copy in ctx_sent + part_sent + full_sent + gate_sent:
        copy.wait_send()
    for level in range(levels):
        wide = 1 << level
        for d in range(2):

            @pl.when(lax.rem(place[d], 2 * wide) == wide - 1)
            def _():
                for k in range(1, wide + 1):
                    map_copy(level, d, k).wait_send()


def on_device(
    n,
    t,
    latent,
    cond,
    context,
    ctx_cond,
    w_mod,
    norm_gain,
    w_query,
    w_key,
    w_value,
    w_outgate,
    w_decay,
    w_beta,
    decay_rate,
    decay_bias,
    extra_decay,
    out_gain,
    w_out,
):
    depth = latent.shape[2]
    span = latent.shape[1]
    heads = w_decay.shape[2]
    inner = heads * HEAD
    chains = 2 * heads
    ctx_len = n * context.shape[1]
    rows = -(-(span + ctx_len) // 128) * 128
    rows_out = span // t
    levels = max(1, (n - 1).bit_length())
    wdb = jnp.concatenate([w_decay.reshape(depth, chains), w_beta.reshape(depth, chains)], axis=1).T
    vmem = pl.BlockSpec(memory_space=pltpu.VMEM)
    smem = pl.BlockSpec(memory_space=pltpu.SMEM)
    hbm = pl.BlockSpec(memory_space=pl.ANY)
    dma = pltpu.SemaphoreType.DMA
    return pl.pallas_call(
        functools.partial(kernel, n, t, heads),
        out_shape=jax.ShapeDtypeStruct((1, rows_out, depth), BF16),
        in_specs=[smem] * 2 + [vmem] * 7 + [hbm] * 7,
        out_specs=vmem,
        scratch_shapes=[
            pltpu.VMEM((span, depth), BF16),
            pltpu.VMEM(w_mod.shape, BF16),
            pltpu.VMEM((4, depth, inner), BF16),
            pltpu.VMEM(w_out.shape, BF16),
            pltpu.VMEM((n,) + context.shape[1:], BF16),
            pltpu.VMEM((n, 2, w_mod.shape[1]), F32),
            pltpu.VMEM((t, 2, w_mod.shape[1]), F32),
            pltpu.VMEM((rows, depth), BF16),
            pltpu.VMEM((8, rows), F32),
            pltpu.VMEM((chains, HEAD, HEAD), F32),
            pltpu.VMEM((chains, HEAD, HEAD), F32),
            pltpu.VMEM((chains, HEAD, HEAD), F32),
            pltpu.VMEM((chains, HEAD, HEAD), F32),
            pltpu.VMEM((levels, 2, 2 * heads, HEAD, HEAD), BF16),
            pltpu.VMEM((levels, 2, 2 * heads, HEAD, HEAD), BF16),
            pltpu.VMEM((t, rows_out, inner), BF16),
            pltpu.VMEM((t, rows_out, inner), BF16),
            dma((7,)),
            dma((n,)),
            dma((n,)),
            dma((n,)),
            dma((n,)),
            dma((t,)),
            dma((t,)),
            dma((levels, 2, n)),
            dma((levels, 2)),
            dma((t,)),
            dma((t,)),
        ],
        compiler_params=pltpu.CompilerParams(
            collective_id=0, has_side_effects=True, vmem_limit_bytes=60 * 1024 * 1024
        ),
    )(
        decay_rate,
        decay_bias,
        cond,
        ctx_cond[None, :],
        context,
        norm_gain[None, :],
        out_gain[None, :],
        wdb,
        extra_decay,
        latent,
        w_mod,
        w_query,
        w_outgate,
        w_key,
        w_value,
        w_out,
    )


def solution(mesh):
    placed = (
        P("dp", "sp", None),
        P("dp", "sp"),
        P("dp", "sp", None),
        P("sp"),
        P("sp", "tp"),
        P(),
        P(None, "tp"),
        P(None, "tp"),
        P(None, "tp"),
        P(None, "tp"),
        P(None, None, "tp"),
        P(None, None, "tp"),
        P(None, "tp"),
        P(None, "tp"),
        P("dp", None, "tp", "sp"),
        P(),
        P(),
    )
    return jax.shard_map(
        functools.partial(on_device, mesh.shape["sp"], mesh.shape["tp"]),
        mesh=mesh,
        in_specs=placed,
        out_specs=P("dp", ("sp", "tp"), None),
        check_vma=False,
    )
```

time: 258 us -> 42.6 us (0.17)
  blocking collectives: 104 us -> 0 us
  matrix products: 68.8 us -> 0 us
  Pallas kernels: 0 us -> 35.9 us
  other arithmetic: 35 us -> 0.64 us
  local copies, waits for them, and re-layouts: 36.3 us -> 5.6 us
  waiting for transfers between devices: 4.89 us -> 0 us
  starting transfers between devices: 3.3 us -> 0 us
    all_gather x6 -> x0, blocking collectives: 83.3 us -> none  [the longest x4 60.9 us: prefix_2(): everything = jax.tree.map(lambda part: lax.all_gather(part, axis), array)]
    dot_general x132 -> x0, matrix products: 68.8 us -> none  [the longest x128 56.8 us: contract_product(): jnp.einsum(einsum_form, left_op, right_op, precision=lax.Precision.HIGHEST)]
    pallas_call x0 -> x1, Pallas kernels: none -> 35.9 us  [on_device(): pl.pallas_call(functools.partial(kernel, n, t, heads), out_shape=jax.Shap...]
    psum x1 -> x0, blocking collectives: 20.4 us -> none  [on_device(): summed = lax.psum(partial_mod, 'sp')]
    concatenate x1 -> x0, local copies, waits for them, and re-layouts: 7.98 us -> none  [on_device(): lat_joined = jnp.concatenate([w_query, w_outgate, ctx_joined], axis=1)]
    mul x13 -> x0, other arithmetic: 7.61 us -> none  [the longest x1 3.21 us: query_terms(): query_decayed = query_blocks * jnp.exp(cumulative)[..., None]]
    eq x11 -> x0, other arithmetic: 5.74 us -> none  [unit_inverse(): upper_half = positions[None, :] // half_width % 2 == 0]
    select_n x11 -> x0, other arithmetic: 5.41 us -> none  [unit_inverse(): positions[:, None] // (2 * half_width)]
  transfers between devices with their start and end apart: 1 -> 0, of which waited for: 1 -> 0; matrix products, arithmetic and copies ran while one was open for 0% -> 0% of each run, Pallas kernels for 0% -> 0%
where the time goes in v1:
time: 42.6 us; the launch traced here: 42.2 us
  Pallas kernels  35.9 us (84%)
  local copies, waits for them, and re-layouts  5.6 us (13%)
  other arithmetic  0.64 us (2%)
    pallas_call x1, Pallas kernels, on_device(): pl.pallas_call(functools.partial(kernel, n, t, heads), out_shape=jax.Shap...  35.9 us
    unnamed x1, local copies, waits for them, and re-layouts  1.62 us
    broadcast_in_dim x1, local copies, waits for them, and re-layouts, on_device(): norm_gain[None, :]  1.28 us
    broadcast_in_dim x1, local copies, waits for them, and re-layouts, on_device(): ctx_cond[None, :]  1.24 us

profile of v1, /device:TPU:0, one launch (start us, length us, event | category | flops | bytes accessed | tf_op | source)
XLA Modules:
  0.0 42.2 jit_solution(18175926261641797636)
XLA Ops:
  0.0 1.2 %broadcast_in_dim.9.ctx_cond_ref = bf16[1,512]{1,0:T(2,128)(2,1)} reshape(bf16[512]{0:T(512)(128)(2,1)} %param.20) | data formatting | bytes 2048 | tf_op jit(solution)/shard_map/broadcast_in_dim | solution.py:500
  1.2 1.3 %broadcast_in_dim.10.gain_ref = bf16[1,2048]{1,0:T(2,128)(2,1)} reshape(bf16[2048]{0:T(1024)(128)(2,1)} %param.22) | data formatting | bytes 8192 | tf_op jit(solution)/shard_map/broadcast_in_dim | solution.py:502
  2.5 0.7 %reshape.6 = bf16[2048,4]{0,1:T(4,128)(2,1)S(1)} reshape(bf16[2048,2,2]{0,2,1:T(2,128)(2,1)} %param.27) | data formatting | bytes 32768 | tf_op jit(solution)/shard_map/reshape | solution.py:453
  3.3 0.7 %reshape.7 = bf16[2048,4]{0,1:T(4,128)(2,1)S(1)} reshape(bf16[2048,2,2]{0,2,1:T(2,128)(2,1)} %param.28) | data formatting | bytes 32768 | tf_op jit(solution)/shard_map/reshape | solution.py:453
  4.0 0.6 %maximum_bitcast_fusion.wdb_ref = bf16[8,2048]{1,0:T(8,128)(2,1)} fusion(bf16[2048,4]{0,1:T(4,128)(2,1)S(1)} %reshape.7, bf16[2048,4]{0,1:T(4,128)(2,1)S(1)} %reshape.6), kind=kLoop, calls=%fused_computation | loop fusion | flops 65536 | bytes 65536 | tf_op jit(solution)/shard_map/transpose | solution.py:453
  4.6 35.9 %shard_map.163 = bf16[1,48,2048]{2,1,0:T(8,128)(2,1)} custom-call(f32[2,2]{1,0:T(2,128)} %rate_ref.1, f32[2,2]{1,0:T(2,128)} %bias_ref.1, bf16[1,512]{1,0:T(2,128)(2,1)} %cond_ref.1, bf16[1,512]{1,0:T(2,128)(2,1)} %broadcast_in_dim.9.ctx_cond_ref, bf16[1,8,2048]{2,1,0:T(8,128)(2,1)} %context_ref.1, bf16[1,2048]{1,0:T(2,128)(2,1)} %broadcast_in_dim.10.gain_ref, ...), custom_call_target="tpu_custom_call" | custom-call | tf_op jit(solution)/shard_map/pallas_call | solution.py:458
  40.6 1.6 %copy.19 = bf16[1,48,2048]{2,1,0:T(8,128)(2,1)} copy(bf16[1,48,2048]{2,1,0:T(8,128)(2,1)} %shard_map.163) | data formatting | bytes 393216

commit v2 on v1

--- a/solution.py
+++ b/solution.py
@@ -48,7 +48,8 @@
     context_ref,
     gain_ref,
     out_gain_ref,
-    wdb_ref,
+    w_decay_ref,
+    w_beta_ref,
     extra_ref,
     latent_hbm,
     w_mod_hbm,
@@ -104,11 +105,6 @@
 
     load_mod = load(0, w_mod_hbm, wm_v)
     load_lat = load(1, latent_hbm.at[0], lat_v)
-    load_w = [
-        load(2 + i, w, w_v.at[i])
-        for i, w in enumerate((w_key_hbm, w_value_hbm, w_query_hbm, w_outgate_hbm))
-    ]
-    load_out = load(6, w_out_hbm, wout_v)
 
     barrier = pltpu.get_barrier_semaphore()
     for k in range(1, n):
@@ -153,9 +149,14 @@
 
     pick = lax.broadcasted_iota(jnp.int32, (8, 1), 0)
     cond_f = silu(cond_ref[...].astype(F32))
-    ctx_cond_f = silu(ctx_cond_ref[...].astype(F32))
+    ctx_cond_f = silu(ctx_cond_ref[...].astype(F32).reshape(1, -1))
     cond_rows = jnp.where(pick == 0, cond_f, jnp.where(pick == 1, ctx_cond_f, 0.0)).astype(BF16)
     load_mod.wait()
+    load_w = [
+        load(2 + i, w, w_v.at[i])
+        for i, w in enumerate((w_key_hbm, w_value_hbm, w_query_hbm, w_outgate_hbm))
+    ]
+    load_out = load(6, w_out_hbm, wout_v)
     part = jnp.dot(cond_rows, wm_v[...], preferred_element_type=F32)
     mod_part[sp] = part[:2]
     part_sent = spread("sp", sp, n, mod_part.at[sp], mod_part, part_send, part_recv)
@@ -166,7 +167,7 @@
     collect("sp", sp, n, ctx_all, ctx_send, ctx_recv)
     ctx = ctx_all[...].astype(F32).reshape(ctx_len, depth)
     ctx_r = lax.rsqrt(jnp.mean(ctx * ctx, axis=-1, keepdims=True) + norm_eps)
-    gain = gain_ref[...].astype(F32)
+    gain = gain_ref[...].astype(F32).reshape(1, depth)
     if rows > span + ctx_len:
         xin[span + ctx_len :, :] = jnp.zeros((rows - span - ctx_len, depth), BF16)
     ext_v[...] = jnp.zeros(ext_v.shape, F32)
@@ -196,8 +197,11 @@
     ctx = ctx_all[...].astype(F32).reshape(ctx_len, depth)
     xin[span : span + ctx_len, :] = (ctx * ctx_r * scale[1:2] + shift[1:2]).astype(BF16)
 
+    wdb = jnp.concatenate(
+        [w[d].astype(F32) for w in (w_decay_ref, w_beta_ref) for d in range(2)], axis=0
+    ).astype(BF16)
     raw_t = lax.dot_general(
-        wdb_ref[...], xin[...], (((1,), (1,)), ((), ())), preferred_element_type=F32
+        wdb, xin[...], (((1,), (1,)), ((), ())), preferred_element_type=F32
     ).astype(BF16).astype(F32)
 
     def project(i):
@@ -303,19 +307,27 @@
             b_map + jnp.where(first, mm(a, ctx_state), 0.0)
         ).astype(BF16)
 
-    def map_copy(level, d, k):
-        wide = 1 << level
-        low_at = heads if 2 * wide == n else 0
-        part_of = pl.ds(low_at, 2 * heads - low_at)
+    def map_copy(level, d, k, which):
+        part_of = pl.ds(which * heads, heads)
         target = lax.rem(sp + k, n) if d == 0 else lax.rem(sp + n - k, n)
         return pltpu.make_async_remote_copy(
             src_ref=send_map.at[level, d, part_of],
             dst_ref=recv_map.at[level, d, part_of],
-            send_sem=map_send.at[level, d, k],
-            recv_sem=map_recv.at[level, d],
+            send_sem=map_send.at[level, d, which, k],
+            recv_sem=map_recv.at[level, d, which],
             device_id={"sp": target},
             device_id_type=MESH,
         )
+
+    def sends_map(level, d):
+        wide = 1 << level
+        at = place[d]
+        return jnp.logical_and(lax.rem(at, 2 * wide) == wide - 1, at >= wide)
+
+    def gets_map(level, d):
+        wide = 1 << level
+        at = place[d]
+        return jnp.logical_and(lax.rem(at, 2 * wide) >= wide, at >= 2 * wide)
 
     levels = (n - 1).bit_length()
 
@@ -328,14 +340,22 @@
                 if level:
                     for h in range(heads):
                         c = d * heads + h
-                        a = own_a[c]
                         send_map[level, d, heads + h] = (
-                            mm(a, pre_b[c]) + own_b[c]
+                            mm(own_a[c], pre_b[c]) + own_b[c]
                         ).astype(BF16)
-                        if 2 * wide != n:
-                            send_map[level, d, h] = mm(a, pre_a[c]).astype(BF16)
-                for k in range(1, wide + 1):
-                    map_copy(level, d, k).start()
+                for k in range(wide, 0, -1):
+                    map_copy(level, d, k, 1).start()
+
+            if 2 * wide < n:
+
+                @pl.when(sends_map(level, d))
+                def _():
+                    if level:
+                        for h in range(heads):
+                            c = d * heads + h
+                            send_map[level, d, h] = mm(own_a[c], pre_a[c]).astype(BF16)
+                    for k in range(wide, 0, -1):
+                        map_copy(level, d, k, 0).start()
 
     def recv_level(level):
         wide = 1 << level
@@ -343,13 +363,19 @@
 
             @pl.when(lax.rem(place[d], 2 * wide) >= wide)
             def _():
-                map_copy(level, d, 1).wait_recv()
+                map_copy(level, d, 1, 1).wait_recv()
                 for h in range(heads):
                     c = d * heads + h
-                    a = pre_a[c]
-                    pre_b[c] = mm(a, recv_map[level, d, heads + h]) + pre_b[c]
-                    if 2 * wide != n:
-                        pre_a[c] = mm(a, recv_map[level, d, h])
+                    pre_b[c] = mm(pre_a[c], recv_map[level, d, heads + h]) + pre_b[c]
+
+            if 2 * wide < n:
+
+                @pl.when(gets_map(level, d))
+                def _():
+                    map_copy(level, d, 1, 0).wait_recv()
+                    for h in range(heads):
+                        c = d * heads + h
+                        pre_a[c] = mm(pre_a[c], recv_map[level, d, h])
 
     if levels:
         send_level(0)
@@ -417,7 +443,14 @@
             @pl.when(lax.rem(place[d], 2 * wide) == wide - 1)
             def _():
                 for k in range(1, wide + 1):
-                    map_copy(level, d, k).wait_send()
+                    map_copy(level, d, k, 1).wait_send()
+
+            if 2 * wide < n:
+
+                @pl.when(sends_map(level, d))
+                def _():
+                    for k in range(1, wide + 1):
+                        map_copy(level, d, k, 0).wait_send()
 
 
 def on_device(
@@ -450,7 +483,6 @@
     rows = -(-(span + ctx_len) // 128) * 128
     rows_out = span // t
     levels = max(1, (n - 1).bit_length())
-    wdb = jnp.concatenate([w_decay.reshape(depth, chains), w_beta.reshape(depth, chains)], axis=1).T
     vmem = pl.BlockSpec(memory_space=pltpu.VMEM)
     smem = pl.BlockSpec(memory_space=pltpu.SMEM)
     hbm = pl.BlockSpec(memory_space=pl.ANY)
@@ -458,7 +490,7 @@
     return pl.pallas_call(
         functools.partial(kernel, n, t, heads),
         out_shape=jax.ShapeDtypeStruct((1, rows_out, depth), BF16),
-        in_specs=[smem] * 2 + [vmem] * 7 + [hbm] * 7,
+        in_specs=[smem] * 2 + [vmem] * 8 + [hbm] * 7,
         out_specs=vmem,
         scratch_shapes=[
             pltpu.VMEM((span, depth), BF16),
@@ -485,8 +517,8 @@
             dma((n,)),
             dma((t,)),
             dma((t,)),
-            dma((levels, 2, n)),
-            dma((levels, 2)),
+            dma((levels, 2, 2, n)),
+            dma((levels, 2, 2)),
             dma((t,)),
             dma((t,)),
         ],
@@ -497,11 +529,12 @@
         decay_rate,
         decay_bias,
         cond,
-        ctx_cond[None, :],
+        ctx_cond,
         context,
-        norm_gain[None, :],
+        norm_gain,
         out_gain[None, :],
-        wdb,
+        jnp.transpose(w_decay, (1, 2, 0)),
+        jnp.transpose(w_beta, (1, 2, 0)),
         extra_decay,
         latent,
         w_mod,

time: 42.6 us -> 36.5 us (0.86)
  local copies, waits for them, and re-layouts: 5.6 us -> 1.62 us
  Pallas kernels: 35.9 us -> 34.7 us
  other arithmetic: 0.64 us -> 0 us
    broadcast_in_dim x2 -> x0, local copies, waits for them, and re-layouts: 2.53 us -> none  [the longest x1 1.28 us: on_device(): norm_gain[None, :]]
    reshape x2 -> x0, local copies, waits for them, and re-layouts: 1.46 us -> none  [the longest x1 0.73 us: on_device(): w_beta.reshape(depth, chains)]
    pallas_call x1, Pallas kernels: 35.9 us -> 34.7 us  [on_device(): pl.pallas_call(functools.partial(kernel, n, t, heads), out_shape=jax.Shap...]
    transpose x1 -> x0, other arithmetic: 0.64 us -> none  [on_device(): jnp.concatenate([w_decay.reshape(depth, chains), w_beta.reshape(depth, ch...]
where the time goes in v2:
time: 36.5 us; the launch traced here: 36.3 us
  Pallas kernels  34.7 us (95%)
  local copies, waits for them, and re-layouts  1.62 us (4%)
    pallas_call x1, Pallas kernels, on_device(): pl.pallas_call(functools.partial(kernel, n, t, heads), out_shape=jax.Shap...  34.7 us
    unnamed x1, local copies, waits for them, and re-layouts  1.62 us

profile of v2, /device:TPU:0, one launch (start us, length us, event | category | flops | bytes accessed | tf_op | source)
XLA Modules:
  0.0 36.3 jit_solution(6261439425951793550)
XLA Ops:
  0.0 34.7 %shard_map.163 = bf16[1,48,2048]{2,1,0:T(8,128)(2,1)} custom-call(f32[2,2]{1,0:T(2,128)} %rate_ref.1, f32[2,2]{1,0:T(2,128)} %bias_ref.1, bf16[1,512]{1,0:T(2,128)(2,1)} %cond_ref.1, bf16[512]{0:T(512)(128)(2,1)} %ctx_cond_ref.1, bf16[1,8,2048]{2,1,0:T(8,128)(2,1)} %context_ref.1, bf16[2048]{0:T(1024)(128)(2,1)} %gain_ref.1, bf16[1,128]{1,0:T(2,128)(2,1)} %bitcast.5, ...), custom_call_target="tpu_custom_call" | custom-call | tf_op jit(solution)/shard_map/pallas_call | solution.py:490
  34.7 1.6 %copy.19 = bf16[1,48,2048]{2,1,0:T(8,128)(2,1)} copy(bf16[1,48,2048]{2,1,0:T(8,128)(2,1)} %shard_map.163) | data formatting | bytes 393216
